TPU v7x, 32 devices: a whole 2x2x4 slice. The times are simulated.
32 devices in a mesh: sp: 4 (over z), fs: 4 (over y, x), tp: 2 (over core).
Axes of the slice: x: 2, y: 2, z: 4, core: 2. Of those that a mesh axis runs over, the one named last changes fastest.
Arguments:
- tokens: bfloat16 [4, 1024, 2048], P('fs', ('sp', 'tp')), may hold values from -6 to 6
- h_gain: float32 [2048], replicated, may hold values from 0.1 to 1.9
- w_qlat: bfloat16 [2048, 768], P(('sp', 'fs')), may hold values from -0.125 to 0.125
- w_kvlat: bfloat16 [2048, 512], P(('sp', 'fs')), may hold values from -0.125 to 0.125
- w_krope: bfloat16 [2048, 32], P(('sp', 'fs')), may hold values from -0.125 to 0.125
- q_gain: float32 [768], replicated, may hold values from 0.3 to 4.5, as said below
- kv_gain: float32 [512], replicated, may hold values from 0.3 to 4.5, as said below
- w_uq: bfloat16 [768, 1536], P(None, 'tp'), may hold values from -0.375 to 0.375
- w_uk: bfloat16 [512, 1024], P(None, 'tp'), may hold values from -0.4375 to 0.4375
- w_uv: bfloat16 [512, 1024], P(None, 'tp'), may hold values from -0.25 to 0.25
- w_convb: bfloat16 [2048, 1024], P(None, 'tp'), may hold values from -0.125 to 0.125
- w_convc: bfloat16 [2048, 1024], P(None, 'tp'), may hold values from -0.125 to 0.125
- w_convx: bfloat16 [2048, 1024], P(None, 'tp'), may hold values from -0.125 to 0.125
- conv_taps: float32 [3, 1024], P(None, 'tp'), may hold values from -3 to 3
- w_out_attn: bfloat16 [1024, 2048], P('tp'), may hold values from -0.125 to 0.125
- w_out_conv: bfloat16 [1024, 2048], P('tp'), may hold values from -0.125 to 0.125
Outputs:
- mixed: bfloat16 [4, 1024, 2048], P('fs', ('sp', 'tp'))
Inputs may be any that keep to these rules, and one draw needn't show every extreme that they name: `q_gain`: positive gains of the query latent's norm. `kv_gain`: positive gains of the key-value latent's norm.
All inputs are finite; a program needn't handle non-finite values.
Results may differ from a plain program's by a relative error of at most 0.017.
The roundings to bfloat16 on the way count: a program that leaves them out, or rounds other values in their place, can miss the bound.
Values may be sent and summed in bfloat16 or wider, within the bound.
A program may use at most 64 MiB of HBM per device.

v0:
```python
import jax
import jax.numpy as jnp
from jax import lax
from jax.sharding import PartitionSpec as P

NOPE = 64
ROPE = 32
VH = 64
KW = 3


EPS = 1e-06
THETA = 10000.0
NEG_START = -1e30


def from_behind(array, axis, by):
    size = lax.axis_size(axis)
    pairs = [(i, i + by) for i in range(size) if 0 <= i + by < size]
    return lax.ppermute(array, axis, pairs)


def normalize(values_in, gain):
    return (
        values_in * lax.rsqrt(jnp.mean(values_in * values_in, axis=-1, keepdims=True) + EPS) * gain
    )


def angle_table(positions, dims):
    inverse = THETA ** (-jnp.arange(0, dims, 2, dtype=jnp.float32) / dims)
    return positions[:, None] * inverse


def rotate(values_in, angles):
    lower_half, upper_half = jnp.split(values_in, 2, axis=-1)
    cosine = jnp.cos(angles)
    sine_part = jnp.sin(angles)
    return jnp.concatenate(
        [
            lower_half * cosine - upper_half * sine_part,
            lower_half * sine_part + upper_half * cosine,
        ],
        axis=-1,
    )


def per_device(
    tokens,
    h_gain,
    w_qlat,
    w_kvlat,
    w_krope,
    q_gain,
    kv_gain,
    w_uq,
    w_uk,
    w_uv,
    w_convb,
    w_convc,
    w_convx,
    conv_taps,
    w_out_attn,
    w_out_conv,
):
    own_rows = lax.all_gather(tokens, "tp", axis=1, tiled=True)
    seq_count = own_rows.shape[0]
    rows_here = own_rows.shape[1]
    flat_count = seq_count * rows_here
    hidden = normalize(own_rows.astype(jnp.float32), h_gain).astype(jnp.bfloat16)
    flat_hidden = hidden.reshape(flat_count, hidden.shape[2])
    groups = lax.axis_size("tp")
    member = lax.axis_index("tp")
    q_cols = w_qlat.shape[1] // groups
    kv_cols = w_kvlat.shape[1] // groups
    rope_cols = w_krope.shape[1] // groups
    q_part = lax.dynamic_slice_in_dim(w_qlat, member * q_cols, q_cols, 1)
    kv_part = lax.dynamic_slice_in_dim(w_kvlat, member * kv_cols, kv_cols, 1)
    rope_part = lax.dynamic_slice_in_dim(w_krope, member * rope_cols, rope_cols, 1)
    whole_q, whole_kv, whole_rope = (
        lax.all_gather(q_part, ("sp", "fs"), axis=0, tiled=True),
        lax.all_gather(kv_part, ("sp", "fs"), axis=0, tiled=True),
        lax.all_gather(rope_part, ("sp", "fs"), axis=0, tiled=True),
    )
    partial_latents = (
        jnp.dot(flat_hidden, whole_q, preferred_element_type=jnp.float32),
        jnp.dot(flat_hidden, whole_kv, preferred_element_type=jnp.float32),
        jnp.dot(flat_hidden, whole_rope, preferred_element_type=jnp.float32),
    )
    query_latent, kv_latent, rope_latent = (
        lax.all_gather(partial_latents[0], "tp", axis=1, tiled=True),
        lax.all_gather(partial_latents[1], "tp", axis=1, tiled=True),
        lax.all_gather(partial_latents[2], "tp", axis=1, tiled=True),
    )
    query_latent = query_latent.reshape(seq_count, rows_here, query_latent.shape[1])
    kv_latent = kv_latent.reshape(seq_count, rows_here, kv_latent.shape[1])
    rope_latent = rope_latent.reshape(seq_count, rows_here, rope_latent.shape[1])
    base = lax.axis_index("sp") * rows_here
    query_pos = base + jnp.arange(rows_here, dtype=jnp.int32)
    angles = angle_table(query_pos.astype(jnp.float32), ROPE)
    query_norm = normalize(query_latent, q_gain).astype(jnp.bfloat16)
    kv_norm = normalize(kv_latent, kv_gain).astype(jnp.bfloat16)
    rope_key = rotate(rope_latent, angles[None]).astype(jnp.bfloat16)
    head_count = w_uk.shape[1] // NOPE
    query = jnp.einsum("sqc,cn->sqn", query_norm, w_uq, preferred_element_type=jnp.float32).reshape(
        seq_count, rows_here, head_count, NOPE + ROPE
    )
    query = jnp.concatenate(
        [query[..., :NOPE], rotate(query[..., NOPE:], angles[None, :, None, :])], axis=-1
    ).astype(jnp.bfloat16)
    query = query.transpose(0, 2, 1, 3)
    score_scale = (NOPE + ROPE) ** (-0.5)
    last_query = base + rows_here - 1
    fold_start = (
        jnp.full((seq_count, head_count, rows_here), NEG_START, jnp.float32),
        jnp.zeros((seq_count, head_count, rows_here), jnp.float32),
        jnp.zeros((seq_count, head_count, rows_here, VH), jnp.float32),
    )
    pieces = (
        lax.all_gather(kv_norm, "sp", axis=1, tiled=True),
        lax.all_gather(rope_key, "sp", axis=1, tiled=True),
    )

    def make_keys():
        key_nope = jnp.einsum(
            "skc,cn->skn", pieces[0], w_uk, preferred_element_type=jnp.float32
        ).astype(jnp.bfloat16)
        value_rows = jnp.einsum(
            "skc,cn->skn", pieces[0], w_uv, preferred_element_type=jnp.float32
        ).astype(jnp.bfloat16)
        return (key_nope, value_rows, pieces[1])

    def compute(state):
        running_max, running_sum, weighted = state
        key_nope, value_rows, rope_piece = make_keys()
        width = rope_piece.shape[1]
        keys = jnp.concatenate(
            [
                key_nope.reshape(seq_count, width, head_count, NOPE),
                jnp.broadcast_to(rope_piece[:, :, None, :], (seq_count, width, head_count, ROPE)),
            ],
            axis=-1,
        )
        scores = (
            jnp.einsum("shqd,skhd->shqk", query, keys, preferred_element_type=jnp.float32)
            * score_scale
        )
        key_pos = jnp.arange(width, dtype=jnp.int32)
        visible = key_pos[None, :] <= query_pos[:, None]
        scores = jnp.where(visible[None, None], scores, -jnp.inf)
        new_max = jnp.maximum(running_max, jnp.max(scores, axis=-1))
        weights = jnp.exp(scores - new_max[..., None])
        new_sum = jnp.sum(weights, axis=-1)
        update = jnp.einsum(
            "shqk,skhv->shqv",
            weights.astype(jnp.bfloat16),
            value_rows.reshape(seq_count, width, head_count, VH),
            preferred_element_type=jnp.float32,
        )
        return (new_max, new_sum, update)

    def keep(state):
        return state

    final = lax.cond(jnp.int32(0) <= last_query, compute, keep, fold_start)
    attn = (
        (final[2] / final[1][..., None])
        .transpose(0, 2, 1, 3)
        .reshape(seq_count, rows_here, head_count * VH)
        .astype(jnp.bfloat16)
    )
    conv_b = jnp.dot(flat_hidden, w_convb, preferred_element_type=jnp.float32).reshape(
        seq_count, rows_here, w_convb.shape[1]
    )
    conv_c = jnp.dot(flat_hidden, w_convc, preferred_element_type=jnp.float32)
    conv_x = jnp.dot(flat_hidden, w_convx, preferred_element_type=jnp.float32)
    conv_in = (conv_c * conv_x).astype(jnp.bfloat16).reshape(seq_count, rows_here, w_convc.shape[1])
    edge_rows = from_behind(conv_in[:, rows_here - (KW - 1) :], "sp", 1)
    padded = jnp.concatenate([edge_rows, conv_in], axis=1).astype(jnp.float32)
    filtered = jnp.zeros(conv_b.shape, jnp.float32)
    for tap in range(KW):
        filtered = filtered + conv_taps[tap] * padded[:, tap : tap + rows_here]
    conv_out = (conv_b * filtered).astype(jnp.bfloat16)
    result = lax.psum_scatter(
        (
            jnp.einsum("sqc,cd->qsd", attn, w_out_attn, preferred_element_type=jnp.float32)
            + jnp.einsum("sqc,cd->qsd", conv_out, w_out_conv, preferred_element_type=jnp.float32)
        ).astype(jnp.bfloat16),
        "tp",
        scatter_dimension=0,
        tiled=True,
    )
    return result.transpose(1, 0, 2)


def solution(mesh):
    in_specs = (
        P("fs", ("sp", "tp"), None),
        P(),
        P(("sp", "fs"), None),
        P(("sp", "fs"), None),
        P(("sp", "fs"), None),
        P(),
        P(),
        P(None, "tp"),
        P(None, "tp"),
        P(None, "tp"),
        P(None, "tp"),
        P(None, "tp"),
        P(None, "tp"),
        P(None, "tp"),
        P("tp", None),
        P("tp", None),
    )
    out_specs = P("fs", ("sp", "tp"), None)
    return jax.shard_map(
        per_device, mesh=mesh, in_specs=in_specs, out_specs=out_specs, check_vma=False
    )
```

profile of v0, /device:TPU:25, one launch (start us, length us, event | category | flops | bytes accessed | tf_op | source)
XLA Modules:
  0.0 198.0 jit_solution(10670061226745212399)
XLA Ops:
  6.5 0.7 all-gather.6.cloned.1.call-update
  7.3 1.5 constant_dynamic-slice_fusion.2
  8.9 1.6 constant_dynamic-slice_fusion
  10.5 1.4 fusion.59
  11.9 0.7 constant_dynamic-slice_fusion.1
  12.6 1.6 copy.22
  14.2 28.5 %all_gather.31 = bf16[2048,16]{0,1:T(8,128)(2,1)} all-gather(bf16[128,16]{0,1:T(8,128)(2,1)S(1)} %constant_dynamic-slice_fusion.1), channel_id=1, replica_groups=mesh['sp'=4,'fs'=4,'tp'=2] {'sp','fs'}, dimensions={0}, use_global_device_ids=true | all-gather | bytes 69632 | tf_op jit(solution)/shard_map/all_gather | solution.py:82
  42.7 0.8 multiply_cosine_fusion
  43.5 1.5 fusion.20
  45.1 2.8 %fusion.49 = f32[256,512]{1,0:T(8,128)S(1)} fusion(bf16[2048,512]{1,0:T(8,128)(2,1)} %param.29, bf16[1,256,2048]{2,1,0:T(8,128)(2,1)} %all-gather.6.cloned.1.call-done, f32[2048]{0:T(1024)S(1)} %copy-done.17, f32[256]{0:T(256)S(1)} %add_rsqrt_fusion.2), kind=kOutput, calls=%fused_computation.82 | convolution fusion | flops 538968064 | bytes 3679232 | tf_op jit(solution)/shard_map/dot_general | solution.py:174
  47.9 0.8 fusion.26
  49.3 1.3 collective-permute-start
  51.0 8.9 %all_gather.32 = f32[256,32]{0,1:T(8,128)S(1)} all-gather(f32[256,16]{0,1:T(8,128)S(1)} %fusion.55), channel_id=1, replica_groups=mesh['sp'=4,'fs'=4,'tp'=2] {'tp'}, dimensions={1}, use_global_device_ids=true | all-gather | bytes 49152 | tf_op jit(solution)/shard_map/all_gather | solution.py:92
  60.1 14.5 %all-gather.8.cloned.1.call-done = bf16[2048,256]{1,0:T(8,128)(2,1)} async-done(((bf16[128,256]{1,0:T(8,128)(2,1)}), bf16[2048,256]{1,0:T(8,128)(2,1)}) %all-gather.8.cloned.1.call-update) | async-done | bytes 1048592 | tf_op jit(solution)/shard_map/all_gather | solution.py:81
  74.6 2.1 %fusion.57 = f32[256,256]{1,0:T(8,128)S(1)} fusion(bf16[2048,256]{1,0:T(8,128)(2,1)} %all-gather.8.cloned.1.call-done, bf16[1,256,2048]{2,1,0:T(8,128)(2,1)} %all-gather.6.cloned.1.call-done, f32[2048]{0:T(1024)} %param.19, f32[256]{0:T(256)} %copy-done.12), kind=kOutput, calls=%fused_computation.85 | convolution fusion | flops 270532608 | bytes 2368512 | tf_op jit(solution)/shard_map/dot_general | solution.py:86
  76.7 4.7 %all_gather.29 = f32[256,512]{1,0:T(8,128)S(1)} all-gather(f32[256,256]{1,0:T(8,128)S(1)} %fusion.57), channel_id=1, replica_groups=mesh['sp'=4,'fs'=4,'tp'=2] {'tp'}, dimensions={1}, use_global_device_ids=true | all-gather | bytes 786432 | tf_op jit(solution)/shard_map/all_gather | solution.py:91
  81.6 0.8 multiply_convert_fusion.1
  82.5 11.1 %all_gather.33 = bf16[1,1024,32]{1,2,0:T(8,128)(2,1)} all-gather(bf16[1,256,32]{1,2,0:T(8,128)(2,1)S(1)} %pad_maximum_fusion), channel_id=1, replica_groups=mesh['sp'=4,'fs'=4,'tp'=2] {'sp'}, dimensions={1}, use_global_device_ids=true | all-gather | bytes 81920 | tf_op jit(solution)/shard_map/all_gather | solution.py:120
  93.5 1.5 maximum_convert_fusion
  95.1 39.4 %all-gather.10.cloned.1.call-done = bf16[2048,384]{1,0:T(8,128)(2,1)} async-done(((bf16[128,384]{1,0:T(8,128)(2,1)}), bf16[2048,384]{1,0:T(8,128)(2,1)}) %all-gather.10.cloned.1.call-update) | async-done | bytes 1572880 | tf_op jit(solution)/shard_map/all_gather | solution.py:80
  134.5 2.5 %fusion.53 = f32[256,384]{1,0:T(8,128)S(1)} fusion(bf16[2048,384]{1,0:T(8,128)(2,1)} %all-gather.10.cloned.1.call-done, bf16[1,256,2048]{2,1,0:T(8,128)(2,1)} %all-gather.6.cloned.1.call-done, f32[2048]{0:T(1024)} %param.19, f32[256]{0:T(256)} %copy-done.12), kind=kOutput, calls=%fused_computation.83 | convolution fusion | flops 404750336 | bytes 3023872 | tf_op jit(solution)/shard_map/dot_general | solution.py:85
  137.0 4.9 %all_gather.35 = f32[256,768]{1,0:T(8,128)S(1)} all-gather(f32[256,384]{1,0:T(8,128)S(1)} %fusion.53), channel_id=1, replica_groups=mesh['sp'=4,'fs'=4,'tp'=2] {'tp'}, dimensions={1}, use_global_device_ids=true | all-gather | bytes 1179648 | tf_op jit(solution)/shard_map/all_gather | solution.py:90
  142.8 21.5 %all-gather.12.cloned.1.call-done = bf16[1024,512]{1,0:T(8,128)(2,1)} async-done(((bf16[256,512]{1,0:T(8,128)(2,1)}), bf16[1024,512]{1,0:T(8,128)(2,1)}) %all-gather.12.cloned.1.call-update) | async-done | bytes 1048592 | tf_op jit(solution)/shard_map/all_gather | solution.py:119
  164.3 8.8 %conditional.1 = (f32[1,8,256]{2,1,0:T(8,128)S(1)}, f32[1,8,256,64]{2,3,1,0:T(8,128)S(1)}) conditional(s32[]{:T(128)} %convert_element_type.97, () %tuple.13, (s32[]{:T(128)}, s32[256]{0:T(256)S(1)}, bf16[1,1024,512]{2,1,0:T(8,128)(2,1)}, bf16[512,512]{1,0:T(8,128)(2,1)}, bf16[1,1024,32]{1,2,0:T(8,128)(2,1)S(1)}, ...), branch_computations={%region_3.0_spmd, %region_4.7_spmd} | conditional | flops 1772353792 | bytes 41929804 | solution.py:164
  164.5 2.1 %convolution_convert_fusion.1 = bf16[1024,512]{0,1:T(8,128)(2,1)S(1)} fusion(bf16[512,512]{1,0:T(8,128)(2,1)} %get-tuple-element.34, bf16[1,1024,512]{2,1,0:T(8,128)(2,1)} %get-tuple-element.23), kind=kOutput, calls=%fused_computation.12 | convolution fusion | flops 537395200 | bytes 2621440 | tf_op jit(solution)/shard_map/cond/branch_1_fun/skc,cn->skn/dot_general | solution.py:124
  166.7 1.8 fusion.2
  168.5 0.8 convolution_convert_fusion
  169.3 2.1 %fusion.9 = f32[1,8,256,64]{2,3,1,0:T(8,128)S(1)} fusion(bf16[1024,8,64]{0,2,1:T(8,128)(2,1)S(1)} %bitcast.107, f32[8,1024,256]{2,1,0:T(8,128)S(1)} %get-tuple-element.37, f32[8,256]{1,0:T(8,128)S(1)} %broadcast_maximum_fusion, pred[256,1024]{0,1:T(8,128)(4,1)S(1)} %iota_compare_fusion), kind=kOutput, calls=%fused_computation.13 | convolution fusion | flops 276824064 | bytes 10231808 | tf_op jit(solution)/shard_map/cond/branch_1_fun/shqk,skhv->shqv/dot_general | solution.py:153
  171.4 1.7 fusion.1
  173.2 2.1 %fusion.60 = f32[256,2048]{1,0:T(8,128)} fusion(bf16[256,512]{0,1:T(8,128)(2,1)S(1)} %bitcast.97, bf16[512,2048]{1,0:T(8,128)(2,1)S(1)} %copy-done), kind=kOutput, calls=%fused_computation.87 | convolution fusion | flops 536870912 | bytes 4456448 | tf_op jit(solution)/shard_map/sqc,cd->qsd/dot_general | solution.py:185
  175.3 5.8 %fusion.19 = bf16[256,1,2048]{2,0,1:T(8,128)(2,1)} fusion(f32[256,2048]{1,0:T(8,128)} %fusion.60, bf16[512,2048]{1,0:T(8,128)(2,1)} %param.33, bf16[2048,512]{1,0:T(8,128)(2,1)} %param.28, f32[1,258,512]{2,1,0:T(8,128)} %maximum_convert_fusion, f32[512]{0:T(512)S(1)} %bitcast.103, f32[512]{0:T(512)S(1)} %bitcast.104, f32[512]{0:T(512)S(1)} %bitcast.102, ...), kind=kOutput, calls=%fused_computation.27 | convolution fusion | flops 1077805056 | bytes 9976832 | tf_op jit(solution)/shard_map/sqc,cd->qsd/dot_general | solution.py:186
  181.1 10.3 %reduce-scatter.2.cloned.1.call-done = bf16[128,1,2048]{2,0,1:T(8,128)(2,1)} async-done(((bf16[256,1,2048]{2,0,1:T(8,128)(2,1)}), bf16[128,1,2048]{2,0,1:T(8,128)(2,1)}) %reduce-scatter.2.cloned.1.call-update) | async-done | bytes 524304 | tf_op jit(solution)/shard_map/reduce_scatter | solution.py:183
  (70 shorter events, 2.8 us)
Async XLA Ops:
  6.5 166.6 %copy-start = (bf16[512,2048]{1,0:T(8,128)(2,1)S(1)}, bf16[512,2048]{1,0:T(8,128)(2,1)}, u32[]{:S(2)}) copy-start(bf16[512,2048]{1,0:T(8,128)(2,1)} %param.32) | copy-start | bytes 6291460
  6.5 37.0 %all-gather.6.cloned.1.call-start = ((), (), s32[]{:S(2)}) async-start(), calls=%async_computation.1 | async-start | bytes 1572864 | tf_op jit(solution)/shard_map/all_gather | solution.py:65
  7.3 37.8 %copy-start.17 = (f32[2048]{0:T(1024)S(1)}, f32[2048]{0:T(1024)}, u32[]{:S(2)}) copy-start(f32[2048]{0:T(1024)} %param.19) | copy-start | bytes 24580
  7.3 67.4 %all-gather.8.cloned.1.call-start = ((), (), s32[]{:S(2)}) async-start(), calls=%async_computation.2 | async-start | bytes 1114112 | tf_op jit(solution)/shard_map/all_gather | solution.py:81
  8.8 125.7 %all-gather.10.cloned.1.call-start = ((), (), s32[]{:S(2)}) async-start(), calls=%async_computation.3 | async-start | bytes 1671168 | tf_op jit(solution)/shard_map/all_gather | solution.py:80
  10.5 153.9 %all-gather.12.cloned.1.call-start = ((), (), s32[]{:S(2)}) async-start(), calls=%async_computation.5 | async-start | bytes 1310720 | tf_op jit(solution)/shard_map/all_gather | solution.py:119
  45.0 5.5 %copy-start.12 = (f32[256]{0:T(256)}, f32[256]{0:T(256)S(1)}, u32[]{:S(2)}) copy-start(f32[256]{0:T(256)S(1)} %add_rsqrt_fusion.2) | copy-start | bytes 3076
  45.0 2.8 %copy-start.1 = (bf16[1,256,2048]{2,1,0:T(8,128)(2,1)S(1)}, bf16[1,256,2048]{2,1,0:T(8,128)(2,1)}, u32[]{:S(2)}) copy-start(bf16[1,256,2048]{2,1,0:T(8,128)(2,1)} %all-gather.6.cloned.1.call-done) | copy-start | bytes 3145732
  45.1 2.9 %copy-start.14 = (bf16[2048,512]{1,0:T(8,128)(2,1)S(1)}, bf16[2048,512]{1,0:T(8,128)(2,1)}, u32[]{:S(2)}) copy-start(bf16[2048,512]{1,0:T(8,128)(2,1)} %param.30) | copy-start | bytes 6291460
  47.9 2.7 %copy-start.4 = (bf16[2048,16]{0,1:T(8,128)(2,1)S(1)}, bf16[2048,16]{0,1:T(8,128)(2,1)}, u32[]{:S(2)}) copy-start(bf16[2048,16]{0,1:T(8,128)(2,1)} %all_gather.31) | copy-start | bytes 196612
  49.3 44.2 %collective-permute-start = (bf16[1,2,512]{2,1,0:T(2,128)(2,1)}, bf16[1,2,512]{2,1,0:T(2,128)(2,1)}, u32[]{:S(2)}, u32[]{:S(2)}) collective-permute-start(bf16[1,2,512]{2,1,0:T(2,128)(2,1)} %slice.37), channel_id=1, source_target_pairs={{0,8},{8,16},{16,24},{1,9},{9,17},{17,25},{2,10},{10,18},{18,26},{... | collective-permute-start | bytes 6152 | tf_op jit(solution)/shard_map/ppermute | solution.py:20
  74.6 6.9 %copy-start.8 = (f32[512]{0:T(512)S(1)}, f32[512]{0:T(512)}, u32[]{:S(2)}) copy-start(f32[512]{0:T(512)} %param.24) | copy-start | bytes 6148
  82.4 109.1 %reduce-scatter.2.cloned.1.call-start = ((), (), s32[]{:S(2)}) async-start(), calls=%async_computation.4 | async-start | bytes 1572864 | tf_op jit(solution)/shard_map/reduce_scatter | solution.py:183
  95.1 47.0 %copy-start.7 = (f32[768]{0:T(1024)S(1)}, f32[768]{0:T(1024)}, u32[]{:S(2)}) copy-start(f32[768]{0:T(1024)} %param.23) | copy-start | bytes 9220
  141.9 0.8 copy-start.5
  141.9 0.8 copy-start.6
  142.1 22.3 %copy-start.3 = (bf16[1,1024,32]{1,2,0:T(8,128)(2,1)S(1)}, bf16[1,1024,32]{1,2,0:T(8,128)(2,1)}, u32[]{:S(2)}) copy-start(bf16[1,1024,32]{1,2,0:T(8,128)(2,1)} %all_gather.33) | copy-start | bytes 196612
  166.7 1.8 copy-start.15
  166.7 1.8 copy-start.16
  173.2 2.1 %copy-start.2 = (bf16[1,256,2048]{2,1,0:T(8,128)(2,1)S(1)}, bf16[1,256,2048]{2,1,0:T(8,128)(2,1)}, u32[]{:S(2)}) copy-start(bf16[1,256,2048]{2,1,0:T(8,128)(2,1)} %all-gather.6.cloned.1.call-done) | copy-start | bytes 3145732
  173.2 2.1 %copy-start.9 = (f32[1,512]{1,0:T(1,128)S(1)}, f32[1,512]{1,0:T(1,128)}, u32[]{:S(2)}) copy-start(f32[1,512]{1,0:T(1,128)} %get-tuple-element.42) | copy-start | bytes 6148
  173.2 2.1 %copy-start.10 = (f32[1,512]{1,0:T(1,128)S(1)}, f32[1,512]{1,0:T(1,128)}, u32[]{:S(2)}) copy-start(f32[1,512]{1,0:T(1,128)} %get-tuple-element.43) | copy-start | bytes 6148
  173.2 2.1 %copy-start.11 = (f32[1,512]{1,0:T(1,128)S(1)}, f32[1,512]{1,0:T(1,128)}, u32[]{:S(2)}) copy-start(f32[1,512]{1,0:T(1,128)} %get-tuple-element.44) | copy-start | bytes 6148
  173.2 2.1 %copy-start.13 = (f32[256]{0:T(256)S(1)}, f32[256]{0:T(256)}, u32[]{:S(2)}) copy-start(f32[256]{0:T(256)} %copy-done.12) | copy-start | bytes 3076
  173.2 2.1 %copy-start.18 = (f32[2048]{0:T(1024)S(1)}, f32[2048]{0:T(1024)}, u32[]{:S(2)}) copy-start(f32[2048]{0:T(1024)} %param.19) | copy-start | bytes 24580
Sparse Core Ops, SparseCore 0:
  8.9 10.7 all-gather.5
  22.4 52.1 all-gather.7
  77.4 57.0 all-gather.9
  135.9 28.3 all-gather.11
  181.3 10.1 reduce-scatter.1
where the time goes:
time: 200 us; the launch traced here: 198 us
  waiting for transfers between devices  86.5 us (43%)
  blocking collectives  58.2 us (29%)
  matrix products  23.8 us (12%)
  between operations  13.5 us (7%)
  local copies, waits for them, and re-layouts  7.5 us (4%)
  other arithmetic  7.07 us (4%)
    all_gather x1, waiting for transfers between devices, per_device(): lax.all_gather(q_part, ('sp', 'fs'), axis=0, tiled=True)  39.4 us
    all_gather x1, blocking collectives, per_device(): lax.all_gather(rope_part, ('sp', 'fs'), axis=0, tiled=True)  28.5 us
    all_gather x1, waiting for transfers between devices, per_device(): lax.all_gather(kv_norm, 'sp', axis=1, tiled=True)  21.5 us
    all_gather x1, waiting for transfers between devices, per_device(): lax.all_gather(kv_part, ('sp', 'fs'), axis=0, tiled=True)  14.5 us
    all_gather x1, blocking collectives, per_device(): lax.all_gather(rope_key, 'sp', axis=1, tiled=True)  11.1 us
    reduce_scatter x1, waiting for transfers between devices, per_device(): lax.psum_scatter((jnp.einsum('sqc,cd->qsd', attn, w_out_attn, preferred_e...  10.3 us
    all_gather x1, blocking collectives, per_device(): lax.all_gather(partial_latents[2], 'tp', axis=1, tiled=True)  8.95 us
    dot_general x1, matrix products, per_device(): jnp.einsum('sqc,cd->qsd', conv_out, w_out_conv, preferred_element_type=jn...  5.8 us
  transfers between devices with their start and end apart: 6, of which 4 were waited for; matrix products, arithmetic and copies ran while one was open for 11% of the time, Pallas kernels for 0%

commit v1 on v0

--- a/solution.py
+++ b/solution.py
@@ -1,6 +1,10 @@
+import functools
+
 import jax
 import jax.numpy as jnp
 from jax import lax
+from jax.experimental import pallas as pl
+from jax.experimental.pallas import tpu as pltpu
 from jax.sharding import PartitionSpec as P
 
 NOPE = 64
@@ -192,6 +196,494 @@
     return result.transpose(1, 0, 2)
 
 
+MESH = pl.DeviceIdType.MESH
+F32 = jnp.float32
+BF16 = jnp.bfloat16
+KV, RK, QL = 0, 1, 2
+
+
+def dot(a, b):
+    return jnp.dot(a, b, preferred_element_type=F32)
+
+
+def dot_t(a, b):
+    return lax.dot_general(a, b, (((1,), (1,)), ((), ())), preferred_element_type=F32)
+
+
+def fused_kernel(
+    ns, nf,
+    tok, h_gain, wq, wkv, wr, q_gain, kv_gain, taps, cos_t, sin_t, cos_q, sin_q,
+    wb_hbm, wc_hbm, wx_hbm, wuq_hbm, wuk_hbm, wuv_hbm, woa_hbm, woc_hbm,
+    out,
+    tok_in, hid, wq_buf, wkv_buf, wr_buf, wb, wc, wx, wuq, wuk, wuv, woa, woc,
+    cbuf, tail_out, tail_in, conv_out,
+    lat_kv, lat_q, kvn, rk, k_buf, v_buf, q_buf, a_buf, part, part_in,
+    load_sem, send_sem, recv_sem, half_sem, tp_send, tp_recv, kz_send, kz_recv, kt_send, kt_recv,
+    tail_sem, out_send, out_recv,
+):
+    z, f, m = lax.axis_index("sp"), lax.axis_index("fs"), lax.axis_index("tp")
+    fx = f + 1 - 2 * (f % 2)
+    fy = (f + 2) % 4
+    fd = fx + 2 - 4 * (fx // 2)
+    other = 1 - m
+    to_x, to_y, to_tp = {"fs": fx}, {"fs": fy}, {"tp": other}
+    to_right, to_left = {"sp": z + 1}, {"sp": z - 1}
+    half_rows, rows = tok.shape[0], hid.shape[0]
+    has_right, has_left = z < ns - 1, z > 0
+    bufs = (wkv_buf, wr_buf, wq_buf)
+    kv_w, q_w = wkv_buf.shape[2], wq_buf.shape[2]
+    kv_own = wkv.at[:, pl.ds(pl.multiple_of(m * kv_w, kv_w), kv_w)]
+    q_own = wq.at[:, pl.ds(pl.multiple_of(m * q_w, q_w), q_w)]
+    owns = (kv_own, wr, q_own)
+    me = z * nf + f
+
+    barrier = pltpu.get_barrier_semaphore()
+    for target in (to_x, to_y, to_tp):
+        pl.semaphore_signal(barrier, inc=1, device_id=target, device_id_type=MESH)
+
+    @pl.when(has_right)
+    def _():
+        pl.semaphore_signal(barrier, inc=1, device_id=to_right, device_id_type=MESH)
+
+    @pl.when(has_left)
+    def _():
+        pl.semaphore_signal(barrier, inc=1, device_id=to_left, device_id_type=MESH)
+
+    loads = [
+        pltpu.make_async_copy(a, b, load_sem.at[i])
+        for i, (a, b) in enumerate(
+            ((wc_hbm, wc), (wx_hbm, wx), (wb_hbm, wb), (wuk_hbm, wuk), (wuv_hbm, wuv),
+             (wuq_hbm, wuq), (woa_hbm, woa), (woc_hbm, woc))
+        )
+    ]
+    for load in loads:
+        load.start()
+    pl.semaphore_wait(barrier, 3 + jnp.where(has_right, 1, 0) + jnp.where(has_left, 1, 0))
+
+    def remote(src, dst, send, recv, target):
+        return pltpu.make_async_remote_copy(
+            src_ref=src, dst_ref=dst, send_sem=send, recv_sem=recv,
+            device_id=target, device_id_type=MESH,
+        )
+
+    def whole(kind, src, slot, lane, target):
+        return remote(
+            src, bufs[kind].at[slot], send_sem.at[kind, slot, lane], recv_sem.at[kind, slot], target
+        )
+
+    def half_of(kind, which):
+        size = bufs[kind].shape[1] // 2
+        return pl.ds(which * size, size)
+
+    def half(kind, slot, which, target):
+        place = bufs[kind].at[slot, half_of(kind, which)]
+        return remote(
+            place, place, send_sem.at[kind, slot, which], half_sem.at[kind, slot, which], target
+        )
+
+    def send_on(kinds, slot, left, right, own=False):
+        for kind in kinds:
+            src = owns[kind] if own else bufs[kind].at[slot]
+            if right is not None:
+                @pl.when(right)
+                def _(kind=kind, src=src):
+                    whole(kind, src, slot, 2, to_right).start()
+            if left is not None:
+                @pl.when(left)
+                def _(kind=kind, src=src):
+                    whole(kind, src, slot, 3, to_left).start()
+            whole(kind, src, slot, 0, to_x).start()
+            whole(kind, src, slot, 1, to_y).start()
+
+    def arrive(kinds, slot):
+        for kind in kinds:
+            whole(kind, bufs[kind].at[slot], slot, 0, to_x).wait_recv()
+
+    def z_step(kinds, d):
+        @pl.when(z - d >= 0)
+        def _():
+            slot = (z - d) * nf + f
+            arrive(kinds, slot)
+            send_on(kinds, slot, None, has_right)
+
+        @pl.when(z + d < ns)
+        def _():
+            slot = (z + d) * nf + f
+            arrive(kinds, slot)
+            send_on(kinds, slot, has_left, None)
+
+    def diag_at(kinds, zo):
+        arrive(kinds, zo * nf + fx)
+        for kind in kinds:
+            half(kind, zo * nf + fx, 0, to_y).start()
+        arrive(kinds, zo * nf + fy)
+        for kind in kinds:
+            half(kind, zo * nf + fy, 1, to_x).start()
+
+    def diag_step(kinds, d):
+        if d == 0:
+            diag_at(kinds, z)
+            return
+
+        @pl.when(z - d >= 0)
+        def _():
+            diag_at(kinds, z - d)
+
+        @pl.when(z + d < ns)
+        def _():
+            diag_at(kinds, z + d)
+
+    def diag_done(kinds):
+        for zo in range(ns):
+            for kind in kinds:
+                for which in range(2):
+                    half(kind, zo * nf + fd, which, to_x).wait_recv()
+
+    first, second = (KV, RK), (QL,)
+    tok_copy = remote(tok, tok_in, tp_send.at[0], tp_recv.at[0], to_tp)
+    tok_copy.start()
+    send_on(first, me, has_left, has_right, own=True)
+    wkv_buf[me] = kv_own[...]
+    wr_buf[me] = wr[...]
+    wq_buf[me] = q_own[...]
+
+    def norm_rows(src, block):
+        data = src[...].astype(F32)
+        hid[pl.ds(pl.multiple_of(block * half_rows, half_rows), half_rows)] = normalize(
+            data, h_gain[...]
+        ).astype(BF16)
+
+    norm_rows(tok, m)
+    tok_copy.wait()
+    norm_rows(tok_in, other)
+    z_step(first, 1)
+
+    width = 256
+    tiles = wc.shape[1] // width
+    pad = 8
+
+    def conv_tile(t, carry):
+        cols = pl.ds(pl.multiple_of(t * width, width), width)
+        made = (dot(hid[...], wc[:, cols]) * dot(hid[...], wx[:, cols])).astype(BF16)
+        cbuf[pl.ds(pad, rows), cols] = made.astype(F32)
+        tail_out[:, cols] = made[rows - tail_out.shape[0] :]
+        return carry
+
+    loads[0].wait()
+    loads[1].wait()
+    diag_step(first, 0)
+    conv_tile(0, 0)
+    z_step(first, 2)
+    diag_step(first, 1)
+    lax.fori_loop(1, tiles, conv_tile, 0)
+    tail_copy = remote(tail_out, tail_in, tail_sem.at[0], tail_sem.at[1], to_right)
+
+    @pl.when(has_right)
+    def _():
+        tail_copy.start()
+
+    for d in range(3, ns):
+        z_step(first, d)
+        diag_step(first, d - 1)
+    send_on(second, me, has_left, has_right, own=True)
+    diag_step(first, ns - 1)
+    z_step(second, 1)
+    diag_step(second, 0)
+
+    @pl.when(has_left)
+    def _():
+        tail_copy.wait_recv()
+        cbuf[0:pad] = tail_in[tail_in.shape[0] - pad :].astype(F32)
+
+    @pl.when(jnp.logical_not(has_left))
+    def _():
+        cbuf[0:pad] = jnp.zeros((pad, cbuf.shape[1]), F32)
+
+    loads[2].wait()
+
+    def gate_tile(t, carry):
+        cols = pl.ds(pl.multiple_of(t * width, width), width)
+        gate = dot(hid[...], wb[:, cols])
+        filtered = jnp.zeros((rows, width), F32)
+        for tap in range(KW):
+            start = pad - (KW - 1) + tap
+            filtered = filtered + taps[tap : tap + 1, cols] * cbuf[pl.ds(start, rows), cols]
+        conv_out[:, cols] = (gate * filtered).astype(BF16)
+        return carry
+
+    lax.fori_loop(0, tiles, gate_tile, 0)
+    z_step(second, 2)
+    diag_step(second, 1)
+
+    diag_done(first)
+    depth = hid.shape[1]
+    lat_kv[m] = dot(hid[...], wkv_buf[...].reshape(depth, kv_w))
+    kv_copy = remote(lat_kv.at[m], lat_kv.at[m], tp_send.at[1], tp_recv.at[1], to_tp)
+    kv_copy.start()
+    w_rope = jnp.concatenate([wr_buf[s] for s in range(ns * nf)], axis=1)
+    rope = dot_t(w_rope, hid[...])
+    low, high = rope[: ROPE // 2], rope[ROPE // 2 :]
+    cos_v, sin_v = cos_t[...], sin_t[...]
+    rk[z] = jnp.concatenate(
+        [low * cos_v - high * sin_v, low * sin_v + high * cos_v], axis=0
+    ).astype(BF16)
+    for d in range(3, ns):
+        z_step(second, d)
+        diag_step(second, d - 1)
+
+    def latent_norm(lat, gain):
+        left, right = lat[0], lat[1]
+        mean = (
+            jnp.sum(left * left, axis=-1, keepdims=True)
+            + jnp.sum(right * right, axis=-1, keepdims=True)
+        ) / (2 * left.shape[1])
+        scale = lax.rsqrt(mean + EPS)
+        cut = left.shape[1]
+        return (
+            (left * scale * gain[:, :cut]).astype(BF16),
+            (right * scale * gain[:, cut:]).astype(BF16),
+        )
+
+    kv_copy.wait()
+    left, right = latent_norm(lat_kv, kv_gain[...])
+    kvn[z, 0] = left
+    kvn[z, 1] = right
+
+    def pass_right(origin):
+        remote(kvn.at[origin, m], kvn.at[origin, m], kz_send.at[0, origin], kz_recv.at[0, origin], to_right).start()
+        remote(rk.at[origin], rk.at[origin], kz_send.at[1, origin], kz_recv.at[1, origin], to_right).start()
+
+    def kz(which, origin):
+        ref = kvn.at[origin, m] if which == 0 else rk.at[origin]
+        return remote(ref, ref, kz_send.at[which, origin], kz_recv.at[which, origin], to_right)
+
+    def kt(origin, part_of):
+        ref = kvn.at[origin, part_of]
+        return remote(ref, ref, kt_send.at[origin], kt_recv.at[origin], to_tp)
+
+    @pl.when(has_right)
+    def _():
+        pass_right(z)
+
+    loads[3].wait()
+    loads[4].wait()
+
+    def make_keys(origin):
+        lhs = jnp.concatenate([kvn[origin, 0], kvn[origin, 1]], axis=1)
+        place = pl.ds(pl.multiple_of(origin * rows, rows), rows)
+
+        def pair(p, carry):
+            cols = pl.ds(pl.multiple_of(p * width, width), width)
+            keys = dot(lhs, wuk[:, cols]).astype(BF16)
+            vals = dot(lhs, wuv[:, cols]).astype(BF16)
+            for i in range(2):
+                k_buf[2 * p + i, place] = keys[:, 128 * i : 128 * (i + 1)]
+                v_buf[2 * p + i, place] = vals[:, 128 * i : 128 * (i + 1)]
+            return carry
+
+        lax.fori_loop(0, wuk.shape[1] // width, pair, 0)
+
+    make_keys(z)
+    for d in range(1, ns):
+        @pl.when(z + d < ns)
+        def _(d=d):
+            place = pl.ds(pl.multiple_of((z + d) * rows, rows), rows)
+            k_buf[:, place] = jnp.zeros((k_buf.shape[0], rows, 128), BF16)
+            v_buf[:, place] = jnp.zeros((v_buf.shape[0], rows, 128), BF16)
+            rk[z + d] = jnp.zeros(rk.shape[1:], BF16)
+
+    diag_step(second, ns - 1)
+
+    def take_keys(d):
+        @pl.when(z - d >= 0)
+        def _():
+            origin = z - d
+            kz(0, origin).wait_recv()
+            kz(1, origin).wait_recv()
+            kt(origin, m).start()
+
+            @pl.when(has_right)
+            def _():
+                pass_right(origin)
+
+    def use_keys(d):
+        @pl.when(z - d >= 0)
+        def _():
+            kt(z - d, other).wait_recv()
+            make_keys(z - d)
+
+    for d in range(1, ns):
+        take_keys(d)
+        if d > 1:
+            use_keys(d - 1)
+    diag_done(second)
+    lat_q[m] = dot(hid[...], wq_buf[...].reshape(depth, q_w))
+    q_copy = remote(lat_q.at[m], lat_q.at[m], tp_send.at[2], tp_recv.at[2], to_tp)
+    q_copy.start()
+    use_keys(ns - 1)
+    q_copy.wait()
+    q_left, q_right = latent_norm(lat_q, q_gain[...])
+    q_norm = jnp.concatenate([q_left, q_right], axis=1)
+    loads[5].wait()
+    head = NOPE + ROPE
+    heads = wuq.shape[1] // head
+    query = dot(q_norm, wuq[...])
+    cos_r, sin_r = cos_q[...], sin_q[...]
+    for h in range(heads):
+        one = query[:, h * head : (h + 1) * head]
+        low, high = one[:, NOPE : NOPE + ROPE // 2], one[:, NOPE + ROPE // 2 :]
+        q_buf[h] = jnp.concatenate(
+            [one[:, :NOPE], low * cos_r - high * sin_r, low * sin_r + high * cos_r], axis=1
+        ).astype(BF16)
+
+    rope_keys = jnp.concatenate([rk[s] for s in range(ns)], axis=1)
+    span = ns * rows
+    visible = lax.broadcasted_iota(jnp.int32, (rows, span), 1) <= (
+        z * rows + lax.broadcasted_iota(jnp.int32, (rows, span), 0)
+    )
+
+    def attend(p, carry):
+        done = []
+        for i in range(2):
+            qh = q_buf[2 * p + i]
+            kh = k_buf[p][:, NOPE * i : NOPE * (i + 1)]
+            vh = v_buf[p][:, VH * i : VH * (i + 1)]
+            scores = dot_t(qh[:, :NOPE], kh) + dot(qh[:, NOPE:], rope_keys)
+            scores = jnp.where(visible, scores * head ** (-0.5), -jnp.inf)
+            weights = jnp.exp(scores - jnp.max(scores, axis=-1, keepdims=True))
+            total = jnp.sum(weights, axis=-1, keepdims=True)
+            done.append(dot(weights.astype(BF16), vh) / total)
+        a_buf[p] = jnp.concatenate(done, axis=1).astype(BF16)
+        return carry
+
+    lax.fori_loop(0, heads // 2, attend, 0)
+    attn = jnp.concatenate([a_buf[p] for p in range(heads // 2)], axis=1)
+    loads[6].wait()
+    loads[7].wait()
+    step = 512
+
+    def out_copy(t):
+        cols = pl.ds(pl.multiple_of(t * step, step), step)
+        return remote(
+            part.at[other, :, cols], part_in.at[:, cols], out_send.at[t], out_recv.at[t], to_tp
+        )
+
+    def project(t, carry):
+        cols = pl.ds(pl.multiple_of(t * step, step), step)
+        term = (dot(attn, woa[:, cols]) + dot(conv_out[...], woc[:, cols])).astype(BF16)
+        part[0, :, cols] = term[:half_rows]
+        part[1, :, cols] = term[half_rows:]
+        out_copy(t).start()
+        return carry
+
+    count = out.shape[1] // step
+    lax.fori_loop(0, count, project, 0)
+
+    def finish(t, carry):
+        cols = pl.ds(pl.multiple_of(t * step, step), step)
+        out_copy(t).wait_recv()
+        out[:, cols] = (part[m, :, cols].astype(F32) + part_in[:, cols].astype(F32)).astype(BF16)
+        return carry
+
+    lax.fori_loop(0, count, finish, 0)
+
+    def sent_slot(kind, slot, left, right):
+        ref = bufs[kind].at[slot]
+        if right is not None:
+            @pl.when(right)
+            def _():
+                whole(kind, ref, slot, 2, to_right).wait_send()
+        if left is not None:
+            @pl.when(left)
+            def _():
+                whole(kind, ref, slot, 3, to_left).wait_send()
+        whole(kind, ref, slot, 0, to_x).wait_send()
+        whole(kind, ref, slot, 1, to_y).wait_send()
+
+    for kind in (KV, RK, QL):
+        sent_slot(kind, me, has_left, has_right)
+        for d in range(1, ns):
+            @pl.when(z - d >= 0)
+            def _(d=d, kind=kind):
+                sent_slot(kind, (z - d) * nf + f, None, has_right)
+
+            @pl.when(z + d < ns)
+            def _(d=d, kind=kind):
+                sent_slot(kind, (z + d) * nf + f, has_left, None)
+        for zo in range(ns):
+            half(kind, zo * nf + fx, 0, to_y).wait_send()
+            half(kind, zo * nf + fy, 1, to_x).wait_send()
+
+    @pl.when(has_right)
+    def _():
+        tail_copy.wait_send()
+        for d in range(ns):
+            @pl.when(z - d >= 0)
+            def _(d=d):
+                kz(0, z - d).wait_send()
+                kz(1, z - d).wait_send()
+
+    for d in range(1, ns):
+        @pl.when(z - d >= 0)
+        def _(d=d):
+            kt(z - d, m).wait_send()
+
+    def sent_out(t, carry):
+        out_copy(t).wait_send()
+        return carry
+
+    lax.fori_loop(0, count, sent_out, 0)
+
+
+def fused_device(
+    ns, nf, tokens, h_gain, w_qlat, w_kvlat, w_krope, q_gain, kv_gain, w_uq, w_uk, w_uv,
+    w_convb, w_convc, w_convx, conv_taps, w_out_attn, w_out_conv,
+):
+    half_rows, depth = tokens.shape[1:]
+    rows = 2 * half_rows
+    slots = ns * nf
+    cut = w_qlat.shape[0]
+    heads = w_uk.shape[1] // NOPE
+    positions = (lax.axis_index("sp") * rows + jnp.arange(rows, dtype=jnp.int32)).astype(F32)
+    angles = angle_table(positions, ROPE)
+    cos_q, sin_q = jnp.cos(angles), jnp.sin(angles)
+    vmem = pl.BlockSpec(memory_space=pltpu.VMEM)
+    anywhere = pl.BlockSpec(memory_space=pl.ANY)
+    V, DMA = pltpu.VMEM, pltpu.SemaphoreType.DMA
+    big = (w_convb, w_convc, w_convx, w_uq, w_uk, w_uv, w_out_attn, w_out_conv)
+    span = ns * rows
+    q_w, kv_w = w_qlat.shape[1] // 2, w_kvlat.shape[1] // 2
+    result = pl.pallas_call(
+        functools.partial(fused_kernel, ns, nf),
+        out_shape=jax.ShapeDtypeStruct((half_rows, depth), BF16),
+        in_specs=[vmem] * 12 + [anywhere] * 8,
+        out_specs=vmem,
+        scratch_shapes=[
+            V((half_rows, depth), BF16), V((rows, depth), BF16),
+            V((slots, cut, q_w), BF16), V((slots, cut, kv_w), BF16), V((slots, ROPE, cut), BF16),
+        ] + [V(w.shape, BF16) for w in big] + [
+            V((rows + 8, w_convc.shape[1]), F32),
+            V((16, w_convc.shape[1]), BF16), V((16, w_convc.shape[1]), BF16),
+            V((rows, w_convc.shape[1]), BF16),
+            V((2, rows, kv_w), F32), V((2, rows, q_w), F32),
+            V((ns, 2, rows, kv_w), BF16), V((ns, ROPE, rows), BF16),
+            V((heads // 2, span, 2 * NOPE), BF16), V((heads // 2, span, 2 * VH), BF16),
+            V((heads, rows, NOPE + ROPE), BF16), V((heads // 2, rows, 2 * VH), BF16),
+            V((2, half_rows, depth), BF16), V((half_rows, depth), BF16),
+            DMA((8,)), DMA((3, slots, 4)), DMA((3, slots)), DMA((3, slots, 2)),
+            DMA((3,)), DMA((3,)), DMA((2, ns)), DMA((2, ns)), DMA((ns,)), DMA((ns,)),
+            DMA((2,)), DMA((4,)), DMA((4,)),
+        ],
+        compiler_params=pltpu.CompilerParams(
+            collective_id=0, has_side_effects=True, vmem_limit_bytes=60 * 1024 * 1024
+        ),
+    )(
+        tokens[0], h_gain[None], w_qlat, w_kvlat, w_krope.T, q_gain[None], kv_gain[None],
+        conv_taps, cos_q.T, sin_q.T, cos_q, sin_q, *big,
+    )
+    return result[None]
+
+
 def solution(mesh):
     in_specs = (
         P("fs", ("sp", "tp"), None),
@@ -212,6 +704,8 @@
         P("tp", None),
     )
     out_specs = P("fs", ("sp", "tp"), None)
+    fits = mesh.shape["tp"] == 2 and mesh.shape["fs"] == 4
+    body = functools.partial(fused_device, mesh.shape["sp"], mesh.shape["fs"]) if fits else per_device
     return jax.shard_map(
-        per_device, mesh=mesh, in_specs=in_specs, out_specs=out_specs, check_vma=False
-    )
+        body, mesh=mesh, in_specs=in_specs, out_specs=out_specs, check_vma=False
+    )

time: 200 us -> 63.9 us (0.32)
  waiting for transfers between devices: 86.5 us -> 0 us
  Pallas kernels: 0 us -> 58.5 us
  blocking collectives: 58.2 us -> 0 us
  matrix products: 23.8 us -> 0 us
  between operations: 13.5 us -> 0.01 us
  other arithmetic: 7.07 us -> 2 us
  local copies, waits for them, and re-layouts: 7.5 us -> 3.17 us
    all_gather x4 -> x0, waiting for transfers between devices: 75.4 us -> none  [the longest x1 39.4 us: per_device(): lax.all_gather(q_part, ('sp', 'fs'), axis=0, tiled=True)]
    pallas_call x0 -> x1, Pallas kernels: none -> 58.5 us  [fused_device(): pl.pallas_call(functools.partial(fused_kernel, ns, nf), out_shape=jax.Sha...]
    all_gather x5 -> x0, blocking collectives: 58.2 us -> none  [the longest x1 28.5 us: per_device(): lax.all_gather(rope_part, ('sp', 'fs'), axis=0, tiled=True)]
    dot_general x12 -> x0, matrix products: 23.8 us -> none  [the longest x1 5.8 us: per_device(): jnp.einsum('sqc,cd->qsd', conv_out, w_out_conv, preferred_element_type=jn...]
    reduce_scatter x1 -> x0, waiting for transfers between devices: 10.3 us -> none  [per_device(): lax.psum_scatter((jnp.einsum('sqc,cd->qsd', attn, w_out_attn, preferred_e...]
    dynamic_slice x3 -> x0, local copies, waits for them, and re-layouts: 3.73 us -> none  [the longest x1 1.56 us: per_device(): q_part = lax.dynamic_slice_in_dim(w_qlat, member * q_cols, q_cols, 1)]
    reduce_sum x4 -> x0, other arithmetic: 3.46 us -> none  [the longest x3 1.75 us: normalize(): jnp.mean(values_in * values_in, axis=-1, keepdims=True) + EPS]
    convert_element_type x4 -> x1, other arithmetic: 2.41 us -> 0.01 us  [fused_device(): (lax.axis_index('sp') * rows + jnp.arange(rows, dtype=jnp.int32)).astype(...]
  transfers between devices with their start and end apart: 6 -> 0, of which waited for: 4 -> 0; matrix products, arithmetic and copies ran while one was open for 11% -> 0% of each run, Pallas kernels for 0% -> 0%
where the time goes in v1:
time: 63.9 us; the launch traced here: 63.6 us
  Pallas kernels  58.5 us (92%)
  local copies, waits for them, and re-layouts  3.17 us (5%)
  other arithmetic  2 us (3%)
    pallas_call x1, Pallas kernels, fused_device(): pl.pallas_call(functools.partial(fused_kernel, ns, nf), out_shape=jax.Sha...  58.5 us
    sin x2, other arithmetic, fused_device(): cos_q, sin_q = (jnp.cos(angles), jnp.sin(angles))  1.98 us
    unnamed x1, local copies, waits for them, and re-layouts  1.88 us
    broadcast_in_dim x1, local copies, waits for them, and re-layouts, fused_device(): q_gain[None]  1.28 us

profile of v1, /device:TPU:25, one launch (start us, length us, event | category | flops | bytes accessed | tf_op | source)
XLA Modules:
  0.0 63.6 jit_solution(7041290491240539648)
XLA Ops:
  0.0 1.3 %broadcast_in_dim.15.q_gain = f32[1,768]{1,0:T(1,128)} reshape(f32[768]{0:T(1024)} %param.21) | data formatting | bytes 6144 | tf_op jit(solution)/shard_map/broadcast_in_dim | solution.py:681
  1.3 0.8 %multiply_sine_fusion.1 = (f32[16,256]{1,0:T(8,128)}, f32[16,256]{1,0:T(8,128)}) fusion(f32[16]{0:T(128)S(1)} %multiply_power_fusion, f32[256]{0:T(256)S(1)} %add_convert_fusion), kind=kLoop, calls=%fused_computation.2 | loop fusion | flops 4096 | bytes 33856 | tf_op jit(solution)/shard_map/sin | solution.py:649
  2.1 1.2 %multiply_sine_fusion = (f32[256,16]{1,0:T(8,128)}, f32[256,16]{1,0:T(8,128)}) fusion(f32[256]{0:T(256)S(1)} %add_convert_fusion, f32[16]{0:T(128)S(1)} %multiply_power_fusion), kind=kLoop, calls=%fused_computation | loop fusion | flops 4096 | bytes 33856 | tf_op jit(solution)/shard_map/sin | solution.py:649
  3.3 58.5 %shard_map.154 = bf16[128,2048]{1,0:T(8,128)(2,1)} custom-call(bf16[128,2048]{1,0:T(8,128)(2,1)} %bitcast.6, f32[1,2048]{1,0:T(1,128)} %bitcast.7, bf16[128,768]{1,0:T(8,128)(2,1)} %wq.1, bf16[128,512]{1,0:T(8,128)(2,1)} %wkv.1, bf16[32,128]{1,0:T(8,128)(2,1)} %bitcast.8, f32[1,768]{1,0:T(1,128)} %broadcast_in_dim.15.q_gain, f32[1,512]{1,0:T(1,128)} %bitcast.9, ...), custom_call_target="tpu_custom_call" | custom-call | tf_op jit(solution)/shard_map/pallas_call | solution.py:656
  61.8 1.9 %copy.19 = bf16[1,128,2048]{2,1,0:T(8,128)(2,1)} copy(bf16[1,128,2048]{2,1,0:T(8,128)(2,1)} %bitcast.5) | data formatting | bytes 1048576
  (2 shorter events, 0.0 us)

commit v2 on v1

--- a/solution.py
+++ b/solution.py
@@ -212,12 +212,12 @@
 
 def fused_kernel(
     ns, nf,
-    tok, h_gain, wq, wkv, wr, q_gain, kv_gain, taps, cos_t, sin_t, cos_q, sin_q,
+    tok, h_gain, wq, wkv, wr, q_gain, kv_gain, taps, inverse,
     wb_hbm, wc_hbm, wx_hbm, wuq_hbm, wuk_hbm, wuv_hbm, woa_hbm, woc_hbm,
     out,
     tok_in, hid, wq_buf, wkv_buf, wr_buf, wb, wc, wx, wuq, wuk, wuv, woa, woc,
     cbuf, tail_out, tail_in, conv_out,
-    lat_kv, lat_q, kvn, rk, k_buf, v_buf, q_buf, a_buf, part, part_in,
+    lat_kv, lat_q, kvn, rk, k_buf, rk_buf, v_buf, wn, wp, cos_r, sin_r, q_rope, q_buf, a_buf, part, part_in,
     load_sem, send_sem, recv_sem, half_sem, tp_send, tp_recv, kz_send, kz_recv, kt_send, kt_recv,
     tail_sem, out_send, out_recv,
 ):
@@ -281,19 +281,20 @@
             place, place, send_sem.at[kind, slot, which], half_sem.at[kind, slot, which], target
         )
 
-    def send_on(kinds, slot, left, right, own=False):
+    def send_on(kinds, slot, left, right, own=False, along=True, across=True):
         for kind in kinds:
             src = owns[kind] if own else bufs[kind].at[slot]
-            if right is not None:
+            if along and right is not None:
                 @pl.when(right)
                 def _(kind=kind, src=src):
                     whole(kind, src, slot, 2, to_right).start()
-            if left is not None:
+            if along and left is not None:
                 @pl.when(left)
                 def _(kind=kind, src=src):
                     whole(kind, src, slot, 3, to_left).start()
-            whole(kind, src, slot, 0, to_x).start()
-            whole(kind, src, slot, 1, to_y).start()
+            if across:
+                whole(kind, src, slot, 0, to_x).start()
+                whole(kind, src, slot, 1, to_y).start()
 
     def arrive(kinds, slot):
         for kind in kinds:
@@ -343,6 +344,7 @@
     tok_copy = remote(tok, tok_in, tp_send.at[0], tp_recv.at[0], to_tp)
     tok_copy.start()
     send_on(first, me, has_left, has_right, own=True)
+    send_on(second, me, None, None, own=True)
     wkv_buf[me] = kv_own[...]
     wr_buf[me] = wr[...]
     wq_buf[me] = q_own[...]
@@ -357,6 +359,7 @@
     tok_copy.wait()
     norm_rows(tok_in, other)
     z_step(first, 1)
+    send_on(second, me, has_left, has_right, own=True, across=False)
 
     width = 256
     tiles = wc.shape[1] // width
@@ -382,38 +385,24 @@
     def _():
         tail_copy.start()
 
+    z_step(second, 1)
     for d in range(3, ns):
         z_step(first, d)
         diag_step(first, d - 1)
-    send_on(second, me, has_left, has_right, own=True)
+    diag_step(second, 0)
     diag_step(first, ns - 1)
-    z_step(second, 1)
-    diag_step(second, 0)
-
-    @pl.when(has_left)
-    def _():
-        tail_copy.wait_recv()
-        cbuf[0:pad] = tail_in[tail_in.shape[0] - pad :].astype(F32)
-
-    @pl.when(jnp.logical_not(has_left))
-    def _():
-        cbuf[0:pad] = jnp.zeros((pad, cbuf.shape[1]), F32)
-
-    loads[2].wait()
-
-    def gate_tile(t, carry):
-        cols = pl.ds(pl.multiple_of(t * width, width), width)
-        gate = dot(hid[...], wb[:, cols])
-        filtered = jnp.zeros((rows, width), F32)
-        for tap in range(KW):
-            start = pad - (KW - 1) + tap
-            filtered = filtered + taps[tap : tap + 1, cols] * cbuf[pl.ds(start, rows), cols]
-        conv_out[:, cols] = (gate * filtered).astype(BF16)
-        return carry
-
-    lax.fori_loop(0, tiles, gate_tile, 0)
+    angles = (
+        z * rows + lax.broadcasted_iota(jnp.int32, cos_r.shape, 0)
+    ).astype(F32) * inverse[...]
+    lanes = lax.broadcasted_iota(jnp.int32, cos_r.shape, 1)
+    cos_r[...] = jnp.cos(angles)
+    sine = jnp.sin(angles)
+    sin_r[...] = jnp.where(lanes < cos_r.shape[1] // 2, -sine, sine)
     z_step(second, 2)
     diag_step(second, 1)
+
+    def rotated(data):
+        return data * cos_r[...] + pltpu.roll(data, data.shape[1] // 2, 1) * sin_r[...]
 
     diag_done(first)
     depth = hid.shape[1]
@@ -421,11 +410,12 @@
     kv_copy = remote(lat_kv.at[m], lat_kv.at[m], tp_send.at[1], tp_recv.at[1], to_tp)
     kv_copy.start()
     w_rope = jnp.concatenate([wr_buf[s] for s in range(ns * nf)], axis=1)
-    rope = dot_t(w_rope, hid[...])
-    low, high = rope[: ROPE // 2], rope[ROPE // 2 :]
-    cos_v, sin_v = cos_t[...], sin_t[...]
+    low, high = w_rope[: ROPE // 2], w_rope[ROPE // 2 :]
+    rope = rotated(dot_t(hid[...], jnp.concatenate([low] * 4 + [high] * 4, axis=0)))
+    rk_buf[0:rows] = rope.astype(BF16)
+    flipped = rope.T
     rk[z] = jnp.concatenate(
-        [low * cos_v - high * sin_v, low * sin_v + high * cos_v], axis=0
+        [flipped[: ROPE // 2], flipped[64 : 64 + ROPE // 2]], axis=0
     ).astype(BF16)
     for d in range(3, ns):
         z_step(second, d)
@@ -449,28 +439,55 @@
     kvn[z, 0] = left
     kvn[z, 1] = right
 
-    def pass_right(origin):
-        remote(kvn.at[origin, m], kvn.at[origin, m], kz_send.at[0, origin], kz_recv.at[0, origin], to_right).start()
-        remote(rk.at[origin], rk.at[origin], kz_send.at[1, origin], kz_recv.at[1, origin], to_right).start()
-
     def kz(which, origin):
-        ref = kvn.at[origin, m] if which == 0 else rk.at[origin]
+        ref = rk.at[origin]
+        if which < 2:
+            ref = kvn.at[origin, m, pl.ds(which * half_rows, half_rows)]
         return remote(ref, ref, kz_send.at[which, origin], kz_recv.at[which, origin], to_right)
 
-    def kt(origin, part_of):
-        ref = kvn.at[origin, part_of]
-        return remote(ref, ref, kt_send.at[origin], kt_recv.at[origin], to_tp)
+    def kt(which, origin, part_of):
+        ref = kvn.at[origin, part_of, pl.ds(which * half_rows, half_rows)]
+        return remote(ref, ref, kt_send.at[which, origin], kt_recv.at[which, origin], to_tp)
 
     @pl.when(has_right)
     def _():
-        pass_right(z)
-
+        for which in range(3):
+            kz(which, z).start()
+
+    @pl.when(has_left)
+    def _():
+        tail_copy.wait_recv()
+        cbuf[0:pad] = tail_in[tail_in.shape[0] - pad :].astype(F32)
+
+    @pl.when(jnp.logical_not(has_left))
+    def _():
+        cbuf[0:pad] = jnp.zeros((pad, cbuf.shape[1]), F32)
+
+    loads[2].wait()
+
+    def gate_tile(t, carry):
+        cols = pl.ds(pl.multiple_of(t * width, width), width)
+        gate = dot(hid[...], wb[:, cols])
+        filtered = jnp.zeros((rows, width), F32)
+        for tap in range(KW):
+            start = pad - (KW - 1) + tap
+            filtered = filtered + taps[tap : tap + 1, cols] * cbuf[pl.ds(start, rows), cols]
+        conv_out[:, cols] = (gate * filtered).astype(BF16)
+        return carry
+
+    lax.fori_loop(0, tiles, gate_tile, 0)
+    diag_step(second, ns - 1)
     loads[3].wait()
     loads[4].wait()
 
-    def make_keys(origin):
+    def make_keys(d):
+        origin = z - d
         lhs = jnp.concatenate([kvn[origin, 0], kvn[origin, 1]], axis=1)
-        place = pl.ds(pl.multiple_of(origin * rows, rows), rows)
+        place = pl.ds(d * rows, rows)
+        if d > 0:
+            got = rk[origin].astype(F32)
+            low, high = got[: ROPE // 2], got[ROPE // 2 :]
+            rk_buf[place] = jnp.concatenate([low] * 4 + [high] * 4, axis=0).T.astype(BF16)
 
         def pair(p, carry):
             cols = pl.ds(pl.multiple_of(p * width, width), width)
@@ -483,80 +500,101 @@
 
         lax.fori_loop(0, wuk.shape[1] // width, pair, 0)
 
-    make_keys(z)
-    for d in range(1, ns):
-        @pl.when(z + d < ns)
-        def _(d=d):
-            place = pl.ds(pl.multiple_of((z + d) * rows, rows), rows)
-            k_buf[:, place] = jnp.zeros((k_buf.shape[0], rows, 128), BF16)
-            v_buf[:, place] = jnp.zeros((v_buf.shape[0], rows, 128), BF16)
-            rk[z + d] = jnp.zeros(rk.shape[1:], BF16)
-
-    diag_step(second, ns - 1)
-
     def take_keys(d):
         @pl.when(z - d >= 0)
         def _():
             origin = z - d
-            kz(0, origin).wait_recv()
-            kz(1, origin).wait_recv()
-            kt(origin, m).start()
-
-            @pl.when(has_right)
-            def _():
-                pass_right(origin)
+            for which in (0, 1, 2):
+                kz(which, origin).wait_recv()
+
+                @pl.when(has_right)
+                def _(which=which):
+                    kz(which, origin).start()
+
+                if which < 2:
+                    kt(which, origin, m).start()
 
     def use_keys(d):
         @pl.when(z - d >= 0)
         def _():
-            kt(z - d, other).wait_recv()
-            make_keys(z - d)
-
-    for d in range(1, ns):
+            kt(0, z - d, other).wait_recv()
+            kt(1, z - d, other).wait_recv()
+            make_keys(d)
+
+    make_keys(0)
+    head = NOPE + ROPE
+    heads = wuq.shape[1] // head
+    loads[5].wait()
+    take_keys(1)
+    for p in range(heads // 2):
+        wn[:, 128 * p : 128 * (p + 1)] = jnp.concatenate(
+            [wuq[:, h * head : h * head + NOPE] for h in (2 * p, 2 * p + 1)], axis=1
+        )
+    for g in range(heads // 4):
+        wp[:, 128 * g : 128 * (g + 1)] = jnp.concatenate(
+            [
+                wuq[:, h * head + NOPE + 16 * i : h * head + NOPE + 16 * (i + 1)]
+                for i in range(2) for h in range(4 * g, 4 * g + 4)
+            ],
+            axis=1,
+        )
+    for d in range(2, ns):
         take_keys(d)
-        if d > 1:
-            use_keys(d - 1)
+        use_keys(d - 1)
     diag_done(second)
     lat_q[m] = dot(hid[...], wq_buf[...].reshape(depth, q_w))
     q_copy = remote(lat_q.at[m], lat_q.at[m], tp_send.at[2], tp_recv.at[2], to_tp)
     q_copy.start()
     use_keys(ns - 1)
     q_copy.wait()
-    q_left, q_right = latent_norm(lat_q, q_gain[...])
+    gains = q_gain[...].reshape(1, -1)
+    q_left, q_right = latent_norm(lat_q, gains)
     q_norm = jnp.concatenate([q_left, q_right], axis=1)
-    loads[5].wait()
-    head = NOPE + ROPE
-    heads = wuq.shape[1] // head
-    query = dot(q_norm, wuq[...])
-    cos_r, sin_r = cos_q[...], sin_q[...]
-    for h in range(heads):
-        one = query[:, h * head : (h + 1) * head]
-        low, high = one[:, NOPE : NOPE + ROPE // 2], one[:, NOPE + ROPE // 2 :]
-        q_buf[h] = jnp.concatenate(
-            [one[:, :NOPE], low * cos_r - high * sin_r, low * sin_r + high * cos_r], axis=1
-        ).astype(BF16)
-
-    rope_keys = jnp.concatenate([rk[s] for s in range(ns)], axis=1)
-    span = ns * rows
-    visible = lax.broadcasted_iota(jnp.int32, (rows, span), 1) <= (
-        z * rows + lax.broadcasted_iota(jnp.int32, (rows, span), 0)
-    )
-
-    def attend(p, carry):
-        done = []
-        for i in range(2):
-            qh = q_buf[2 * p + i]
-            kh = k_buf[p][:, NOPE * i : NOPE * (i + 1)]
-            vh = v_buf[p][:, VH * i : VH * (i + 1)]
-            scores = dot_t(qh[:, :NOPE], kh) + dot(qh[:, NOPE:], rope_keys)
-            scores = jnp.where(visible, scores * head ** (-0.5), -jnp.inf)
-            weights = jnp.exp(scores - jnp.max(scores, axis=-1, keepdims=True))
-            total = jnp.sum(weights, axis=-1, keepdims=True)
-            done.append(dot(weights.astype(BF16), vh) / total)
-        a_buf[p] = jnp.concatenate(done, axis=1).astype(BF16)
-        return carry
-
-    lax.fori_loop(0, heads // 2, attend, 0)
+    nope = dot(q_norm, wn[...])
+    roped = dot(q_norm, wp[...])
+    for p in range(heads // 2):
+        q_buf[p] = nope[:, 128 * p : 128 * (p + 1)].astype(BF16)
+    for g in range(heads // 4):
+        q_rope[g] = rotated(roped[:, 128 * g : 128 * (g + 1)]).astype(BF16)
+
+    lane = lax.broadcasted_iota(jnp.int32, (rows, 128), 1)
+    factor = head ** (-0.5) * 1.4426950408889634
+
+    def attend(blocks):
+        span = blocks * rows
+        seen = lax.broadcasted_iota(jnp.int32, (rows, rows), 1) <= (
+            lax.broadcasted_iota(jnp.int32, (rows, rows), 0)
+        )
+
+        def pair(p, carry):
+            keys = jnp.concatenate([k_buf[p, 0:span], rk_buf[0:span]], axis=1)
+            vals = v_buf[p, 0:span]
+            nope = q_buf[p].astype(F32)
+            roped = q_rope[p // 2].astype(F32)
+            done = []
+            for i in range(2):
+                mine = jnp.where(lane // NOPE == i, nope, 0.0)
+                turn = jnp.where((lane // 16) % 4 == (2 * p + i) % 4, roped, 0.0)
+                scores = dot_t(jnp.concatenate([mine, turn], axis=1).astype(BF16), keys)
+                near = jnp.where(seen, scores[:, :rows], -jnp.inf)
+                if blocks > 1:
+                    scores = jnp.concatenate([near, scores[:, rows:]], axis=1)
+                else:
+                    scores = near
+                largest = jnp.max(scores, axis=-1, keepdims=True)
+                weights = jnp.exp2((scores - largest) * factor)
+                total = jnp.sum(weights, axis=-1, keepdims=True)
+                done.append(dot(weights.astype(BF16), vals) / total)
+            a_buf[p] = jnp.where(lane < VH, done[0], done[1]).astype(BF16)
+            return carry
+
+        lax.fori_loop(0, heads // 2, pair, 0)
+
+    for d in range(ns):
+        @pl.when(z == d)
+        def _(d=d):
+            attend(d + 1)
+
     attn = jnp.concatenate([a_buf[p] for p in range(heads // 2)], axis=1)
     loads[6].wait()
     loads[7].wait()
@@ -620,13 +658,14 @@
         for d in range(ns):
             @pl.when(z - d >= 0)
             def _(d=d):
-                kz(0, z - d).wait_send()
-                kz(1, z - d).wait_send()
+                for which in range(3):
+                    kz(which, z - d).wait_send()
 
     for d in range(1, ns):
         @pl.when(z - d >= 0)
         def _(d=d):
-            kt(z - d, m).wait_send()
+            kt(0, z - d, m).wait_send()
+            kt(1, z - d, m).wait_send()
 
     def sent_out(t, carry):
         out_copy(t).wait_send()
@@ -644,9 +683,7 @@
     slots = ns * nf
     cut = w_qlat.shape[0]
     heads = w_uk.shape[1] // NOPE
-    positions = (lax.axis_index("sp") * rows + jnp.arange(rows, dtype=jnp.int32)).astype(F32)
-    angles = angle_table(positions, ROPE)
-    cos_q, sin_q = jnp.cos(angles), jnp.sin(angles)
+    inverse = jnp.tile(THETA ** (-jnp.arange(0, ROPE, 2, dtype=F32) / ROPE), 8)[None]
     vmem = pl.BlockSpec(memory_space=pltpu.VMEM)
     anywhere = pl.BlockSpec(memory_space=pl.ANY)
     V, DMA = pltpu.VMEM, pltpu.SemaphoreType.DMA
@@ -656,7 +693,7 @@
     result = pl.pallas_call(
         functools.partial(fused_kernel, ns, nf),
         out_shape=jax.ShapeDtypeStruct((half_rows, depth), BF16),
-        in_specs=[vmem] * 12 + [anywhere] * 8,
+        in_specs=[vmem] * 9 + [anywhere] * 8,
         out_specs=vmem,
         scratch_shapes=[
             V((half_rows, depth), BF16), V((rows, depth), BF16),
@@ -667,19 +704,23 @@
             V((rows, w_convc.shape[1]), BF16),
             V((2, rows, kv_w), F32), V((2, rows, q_w), F32),
             V((ns, 2, rows, kv_w), BF16), V((ns, ROPE, rows), BF16),
-            V((heads // 2, span, 2 * NOPE), BF16), V((heads // 2, span, 2 * VH), BF16),
-            V((heads, rows, NOPE + ROPE), BF16), V((heads // 2, rows, 2 * VH), BF16),
+            V((heads // 2, span, 2 * NOPE), BF16), V((span, 128), BF16),
+            V((heads // 2, span, 2 * VH), BF16),
+            V((w_uq.shape[0], heads * NOPE), BF16), V((w_uq.shape[0], heads * ROPE), BF16),
+            V((rows, 128), F32), V((rows, 128), F32),
+            V((heads // 4, rows, 128), BF16), V((heads // 2, rows, 2 * NOPE), BF16),
+            V((heads // 2, rows, 2 * VH), BF16),
             V((2, half_rows, depth), BF16), V((half_rows, depth), BF16),
             DMA((8,)), DMA((3, slots, 4)), DMA((3, slots)), DMA((3, slots, 2)),
-            DMA((3,)), DMA((3,)), DMA((2, ns)), DMA((2, ns)), DMA((ns,)), DMA((ns,)),
+            DMA((3,)), DMA((3,)), DMA((3, ns)), DMA((3, ns)), DMA((2, ns)), DMA((2, ns)),
             DMA((2,)), DMA((4,)), DMA((4,)),
         ],
         compiler_params=pltpu.CompilerParams(
             collective_id=0, has_side_effects=True, vmem_limit_bytes=60 * 1024 * 1024
         ),
     )(
-        tokens[0], h_gain[None], w_qlat, w_kvlat, w_krope.T, q_gain[None], kv_gain[None],
-        conv_taps, cos_q.T, sin_q.T, cos_q, sin_q, *big,
+        tokens[0], h_gain[None], w_qlat, w_kvlat, w_krope.T, q_gain, kv_gain[None],
+        conv_taps, inverse, *big,
     )
     return result[None]
 

time: 63.9 us -> 54.1 us (0.85)
  Pallas kernels: 58.5 us -> 51.4 us
  other arithmetic: 2 us -> 0.01 us
  local copies, waits for them, and re-layouts: 3.17 us -> 2.48 us
    pallas_call x1, Pallas kernels: 58.5 us -> 51.4 us  [fused_device(): pl.pallas_call(functools.partial(fused_kernel, ns, nf), out_shape=jax.Sha...]
    sin x2 -> x0, other arithmetic: 1.98 us -> none  [fused_device(): cos_q, sin_q = (jnp.cos(angles), jnp.sin(angles))]
    broadcast_in_dim x1 -> x0, local copies, waits for them, and re-layouts: 1.28 us -> none  [fused_device(): q_gain[None]]
where the time goes in v2:
time: 54.1 us; the launch traced here: 53.9 us
  Pallas kernels  51.4 us (95%)
  local copies, waits for them, and re-layouts  2.48 us (5%)
    pallas_call x1, Pallas kernels, fused_device(): pl.pallas_call(functools.partial(fused_kernel, ns, nf), out_shape=jax.Sha...  51.4 us
    unnamed x1, local copies, waits for them, and re-layouts  1.88 us

profile of v2, /device:TPU:25, one launch (start us, length us, event | category | flops | bytes accessed | tf_op | source)
XLA Modules:
  0.0 53.9 jit_solution(15907426772191661901)
XLA Ops:
  0.0 0.6 %broadcast_in_dim_tile.3.inverse = f32[1,128]{1,0:T(1,128)} reshape(f32[8,16]{1,0:T(8,128)S(1)} %tile.2) | data formatting | bytes 1024 | tf_op jit(solution)/shard_map/broadcast_in_dim;tile | solution.py:686
  0.6 51.4 %shard_map.154 = bf16[128,2048]{1,0:T(8,128)(2,1)} custom-call(bf16[128,2048]{1,0:T(8,128)(2,1)} %bitcast.6, f32[1,2048]{1,0:T(1,128)} %bitcast.7, bf16[128,768]{1,0:T(8,128)(2,1)} %wq.1, bf16[128,512]{1,0:T(8,128)(2,1)} %wkv.1, bf16[32,128]{1,0:T(8,128)(2,1)} %bitcast.8, f32[768]{0:T(1024)} %q_gain.1, f32[1,512]{1,0:T(1,128)} %bitcast.9, f32[3,512]{1,0:T(4,128)} %taps.1, ...), custom_call_target="tpu_custom_call" | custom-call | tf_op jit(solution)/shard_map/pallas_call | solution.py:693
  52.0 1.9 %copy.18 = bf16[1,128,2048]{2,1,0:T(8,128)(2,1)} copy(bf16[1,128,2048]{2,1,0:T(8,128)(2,1)} %bitcast.5) | data formatting | bytes 1048576
  (2 shorter events, 0.0 us)

commit v3 on v2

--- a/solution.py
+++ b/solution.py
@@ -538,14 +538,15 @@
             ],
             axis=1,
         )
-    for d in range(2, ns):
+    for d in range(2, ns - 1):
         take_keys(d)
         use_keys(d - 1)
     diag_done(second)
     lat_q[m] = dot(hid[...], wq_buf[...].reshape(depth, q_w))
     q_copy = remote(lat_q.at[m], lat_q.at[m], tp_send.at[2], tp_recv.at[2], to_tp)
     q_copy.start()
-    use_keys(ns - 1)
+    if ns > 2:
+        use_keys(ns - 2)
     q_copy.wait()
     gains = q_gain[...].reshape(1, -1)
     q_left, q_right = latent_norm(lat_q, gains)
@@ -556,6 +557,9 @@
         q_buf[p] = nope[:, 128 * p : 128 * (p + 1)].astype(BF16)
     for g in range(heads // 4):
         q_rope[g] = rotated(roped[:, 128 * g : 128 * (g + 1)]).astype(BF16)
+    if ns > 2:
+        take_keys(ns - 1)
+    use_keys(ns - 1)
 
     lane = lax.broadcasted_iota(jnp.int32, (rows, 128), 1)
     factor = head ** (-0.5) * 1.4426950408889634

time: 54.1 us -> 53 us (0.980)
  Pallas kernels: 51.4 us -> 50.2 us
    pallas_call x1, Pallas kernels: 51.4 us -> 50.2 us  [fused_device(): pl.pallas_call(functools.partial(fused_kernel, ns, nf), out_shape=jax.Sha...]
where the time goes in v3:
time: 53 us; the launch traced here: 52.7 us
  Pallas kernels  50.2 us (95%)
  local copies, waits for them, and re-layouts  2.48 us (5%)
    pallas_call x1, Pallas kernels, fused_device(): pl.pallas_call(functools.partial(fused_kernel, ns, nf), out_shape=jax.Sha...  50.2 us
    unnamed x1, local copies, waits for them, and re-layouts  1.88 us

profile of v3, /device:TPU:25, one launch (start us, length us, event | category | flops | bytes accessed | tf_op | source)
XLA Modules:
  0.0 52.7 jit_solution(3692195620686528432)
XLA Ops:
  0.0 0.6 %broadcast_in_dim_tile.3.inverse = f32[1,128]{1,0:T(1,128)} reshape(f32[8,16]{1,0:T(8,128)S(1)} %tile.2) | data formatting | bytes 1024 | tf_op jit(solution)/shard_map/broadcast_in_dim;tile | solution.py:690
  0.6 50.2 %shard_map.154 = bf16[128,2048]{1,0:T(8,128)(2,1)} custom-call(bf16[128,2048]{1,0:T(8,128)(2,1)} %bitcast.6, f32[1,2048]{1,0:T(1,128)} %bitcast.7, bf16[128,768]{1,0:T(8,128)(2,1)} %wq.1, bf16[128,512]{1,0:T(8,128)(2,1)} %wkv.1, bf16[32,128]{1,0:T(8,128)(2,1)} %bitcast.8, f32[768]{0:T(1024)} %q_gain.1, f32[1,512]{1,0:T(1,128)} %bitcast.9, f32[3,512]{1,0:T(4,128)} %taps.1, ...), custom_call_target="tpu_custom_call" | custom-call | tf_op jit(solution)/shard_map/pallas_call | solution.py:697
  50.9 1.9 %copy.18 = bf16[1,128,2048]{2,1,0:T(8,128)(2,1)} copy(bf16[1,128,2048]{2,1,0:T(8,128)(2,1)} %bitcast.5) | data formatting | bytes 1048576
  (2 shorter events, 0.0 us)
